TPU v7x, 32 devices: a whole 2x2x4 slice. The times are simulated.
32 devices in a mesh: fs: 8 (over z, y), tp: 4 (over x, core).
Axes of the slice: x: 2, y: 2, z: 4, core: 2. Of those that a mesh axis runs over, the one named last changes fastest.
Arguments:
- saved_input: bfloat16 [49152, 2048], P(('fs', 'tp')), may hold values from -6 to 6
- key_cot: bfloat16 [49152, 1024], P(('fs', 'tp')), may hold values from -0.042143017 to 0.042143017
- mixed_out: bfloat16 [49152, 1024], P(('fs', 'tp')), may hold values from -6 to 6
- out_cot: bfloat16 [49152, 2048], P(('fs', 'tp')), may hold values from -0.042143017 to 0.042143017
- key_weight: float32 [2048, 1024], P('fs', 'tp'), may hold values from -0.125 to 0.125
- out_weight: float32 [1024, 2048], P('tp', 'fs'), may hold values from -0.1875 to 0.1875
- bases: bfloat16 [2, 1024, 512], replicated, may hold values from -0.1875 to 0.1875
- first_moment: float32 [2, 2048, 512], P(None, 'fs', 'tp'), may hold values from -64 to 64
- second_moment: float32 [2, 2048, 512], P(None, 'fs', 'tp'), may hold values from 0.25 to 4
Outputs:
- key_weight_new: float32 [2048, 1024], P('fs', 'tp')
- out_weight_new: float32 [1024, 2048], P('tp', 'fs')
- key_step: float32 [2048, 1024], P('fs', 'tp')
- out_step: float32 [1024, 2048], P('tp', 'fs')
- first_new: float32 [2, 2048, 512], P(None, 'fs', 'tp')
- second_new: float32 [2, 2048, 512], P(None, 'fs', 'tp')
- key_copy: bfloat16 [2048, 1024], P(None, 'tp')
- out_copy: bfloat16 [1024, 2048], P('tp')
All inputs are finite; a program needn't handle non-finite values.
Results may differ from a plain program's by a relative error of at most 0.0032.
Values may be sent and summed in bfloat16 or wider, within the bound.
A program may use at most 128 MiB of HBM per device.

v0:
```python
import jax
import jax.numpy as jnp
from jax import lax
from jax.sharding import PartitionSpec as P

D = 2048
RANK = 512


highest = lax.Precision.HIGHEST
first_decay = 0.8
second_decay = 0.9
learn_rate = 0.01


def tokens_first(left, right, precision=None):
    return lax.dot_general(
        left,
        right,
        (((0,), (0,)), ((), ())),
        preferred_element_type=jnp.float32,
        precision=precision,
    )


def split_pair(mapped):
    upper = mapped.astype(jnp.bfloat16)
    lower = (mapped - upper.astype(jnp.float32)).astype(jnp.bfloat16)
    return jnp.concatenate((upper, lower), axis=1)


def body(
    saved_input,
    key_cot,
    mixed_out,
    out_cot,
    key_weight,
    out_weight,
    bases,
    first_moment,
    second_moment,
):
    col_share = key_weight.shape[1]
    rank_width = bases.shape[2]
    bases_wide = bases.astype(jnp.float32)
    local_bases = lax.dynamic_slice_in_dim(
        bases_wide, lax.axis_index("tp") * col_share, col_share, 1
    )
    key_mapped = split_pair(jnp.dot(key_cot, bases[0], preferred_element_type=jnp.float32))
    out_mapped = split_pair(jnp.dot(mixed_out, bases[1], preferred_element_type=jnp.float32))
    key_both = tokens_first(saved_input, key_mapped)
    out_both = tokens_first(out_cot, out_mapped)
    key_low = key_both[:, :rank_width] + key_both[:, rank_width:]
    out_low = out_both[:, :rank_width] + out_both[:, rank_width:]
    partial_low = lax.psum_scatter(
        jnp.stack((key_low, out_low), axis=1), "fs", scatter_dimension=0, tiled=True
    )
    reduced = lax.psum_scatter(partial_low, "tp", scatter_dimension=2, tiled=True)
    low_pair = jnp.transpose(reduced, (1, 0, 2))
    first_new = first_decay * first_moment + (1.0 - first_decay) * low_pair
    second_new = second_decay * second_moment + (1.0 - second_decay) * low_pair * low_pair
    direction = first_new / jnp.sqrt(second_new)
    square_sums = lax.psum(jnp.sum(direction * direction, axis=(1, 2)), ("fs", "tp"))
    scales = lax.rsqrt(square_sums / (D * RANK) + 1.0)
    projected = jnp.einsum(
        "mrq,mkq->mrk",
        lax.all_gather(direction, "tp", axis=2, tiled=True),
        local_bases,
        precision=highest,
    )
    scaled = projected * scales[:, None, None]
    key_step = scaled[0]
    out_step = scaled[1].T
    key_new = key_weight - learn_rate * key_step
    out_new = out_weight - learn_rate * out_step
    copies = jnp.stack((key_new.astype(jnp.bfloat16), out_new.T.astype(jnp.bfloat16)))
    gathered = lax.all_gather(copies, "fs", axis=1, tiled=True)
    return (key_new, out_new, key_step, out_step, first_new, second_new, gathered[0], gathered[1].T)


def solution(mesh):
    placed = (
        P(("fs", "tp"), None),
        P(("fs", "tp"), None),
        P(("fs", "tp"), None),
        P(("fs", "tp"), None),
        P("fs", "tp"),
        P("tp", "fs"),
        P(),
        P(None, "fs", "tp"),
        P(None, "fs", "tp"),
    )
    return jax.shard_map(
        body,
        mesh=mesh,
        in_specs=placed,
        out_specs=(
            P("fs", "tp"),
            P("tp", "fs"),
            P("fs", "tp"),
            P("tp", "fs"),
            P(None, "fs", "tp"),
            P(None, "fs", "tp"),
            P(None, "tp"),
            P("tp", None),
        ),
        check_vma=False,
    )
```

profile of v0, /device:TPU:0, one launch (start us, length us, event | category | flops | bytes accessed | tf_op | source)
XLA Modules:
  0.0 334.4 jit_solution(628307181880223142)
XLA Ops:
  7.2 0.0 reduce-scatter.3.cloned.1.call-start
  7.2 1.8 copy-done
  9.1 3.2 subtract_convert_fusion.1
  12.4 1.9 subtract_convert_fusion
  14.3 9.7 %convolution_bitcast_fusion.1 = f32[2048,1024]{0,1:T(8,128)} fusion(bf16[1536,2048]{1,0:T(8,128)(2,1)S(1)} %bitcast.53, bf16[1536,512]{0,1:T(8,128)(2,1)S(1)} %get-tuple-element.25, bf16[1536,512]{0,1:T(8,128)(2,1)S(1)} %get-tuple-element.26), kind=kOutput, calls=%fused_computation.2 | convolution fusion | flops 6448742400 | bytes 17825792 | tf_op jit(solution)/shard_map/dot_general | solution.py:17
  24.0 9.7 %convolution_bitcast_fusion = f32[2048,1024]{0,1:T(8,128)} fusion(bf16[1536,2048]{1,0:T(8,128)(2,1)S(1)} %bitcast.55, bf16[1536,512]{0,1:T(8,128)(2,1)S(1)} %get-tuple-element.27, bf16[1536,512]{0,1:T(8,128)(2,1)S(1)} %get-tuple-element.28), kind=kOutput, calls=%fused_computation.1 | convolution fusion | flops 6448742400 | bytes 17825792 | tf_op jit(solution)/shard_map/dot_general | solution.py:17
  33.7 10.0 %fusion = (f32[2048,1,512]{0,2,1:T(8,128)S(1)}, f32[2048,1,512]{0,2,1:T(8,128)}) fusion(f32[2048,1024]{0,1:T(8,128)} %convolution_bitcast_fusion, f32[2048,1024]{0,1:T(8,128)} %convolution_bitcast_fusion.1), kind=kLoop, calls=%fused_computation.4 | loop fusion | flops 2097152 | bytes 25165824 | tf_op jit(solution)/shard_map/stack | solution.py:56
  43.7 6.3 %pad_maximum_fusion = f32[2048,2,512]{0,2,1:T(8,128)} fusion(f32[2048,1,512]{0,2,1:T(8,128)S(1)} %get-tuple-element.31, f32[2048,1,512]{0,2,1:T(8,128)} %get-tuple-element.32), kind=kLoop, calls=%fused_computation | loop fusion | flops 2097152 | bytes 16777216 | tf_op jit(solution)/shard_map/stack | solution.py:56
  50.0 0.0 reduce-scatter.3.cloned.1.call-update
  50.1 0.2 reduce-scatter.5.cloned.1.call-start
  50.3 150.5 %reduce-scatter.3.cloned.1.call-done = f32[256,2,512]{0,2,1:T(8,128)} async-done(((f32[2048,2,512]{0,2,1:T(8,128)}), f32[256,2,512]{0,2,1:T(8,128)}) %reduce-scatter.3.cloned.1.call-update) | async-done | bytes 1048592 | tf_op jit(solution)/shard_map/reduce_scatter | solution.py:55
  200.8 0.0 reduce-scatter.5.cloned.1.call-update
  200.8 0.0 all-gather.3.cloned.1.call-start
  200.9 0.1 copy.17
  201.0 0.1 copy.18
  201.1 26.1 %reduce-scatter.5.cloned.1.call-done = f32[256,2,128]{0,2,1:T(8,128)} async-done(((f32[256,2,512]{0,2,1:T(8,128)}), f32[256,2,128]{0,2,1:T(8,128)}) %reduce-scatter.5.cloned.1.call-update) | async-done | bytes 262160 | tf_op jit(solution)/shard_map/reduce_scatter | solution.py:58
  227.2 1.8 multiply_reduce_fusion
  229.0 0.0 all-gather.3.cloned.1.call-update
  229.0 0.0 all-gather.5.cloned.1.call-start
  229.1 0.1 copy.21
  229.2 39.6 %psum.7 = f32[2]{0:T(128)S(1)} all-reduce(f32[2]{0:T(128)S(1)} %get-tuple-element.21), channel_id=1, replica_groups=mesh['fs'=8,'tp'=4] {'fs','tp'}, use_global_device_ids=true, to_apply=%region_3.0 | all-reduce | flops 2 | bytes 16 | tf_op jit(solution)/shard_map/psum | solution.py:63
  268.8 2.4 convolution_multiply_fusion
  271.2 0.8 convert_bitcast_fusion.1
  272.1 0.7 pad_maximum_fusion.1
  272.8 0.0 all-gather.5.cloned.1.call-update
  272.8 0.8 copy.24
  273.7 0.8 copy.25
  274.5 0.8 copy.22
  275.4 0.8 copy.23
  276.2 46.4 %all-gather.5.cloned.1.call-done = bf16[2,2048,256]{2,1,0:T(8,128)(2,1)} async-done(((bf16[2,256,256]{2,1,0:T(8,128)(2,1)}), bf16[2,2048,256]{2,1,0:T(8,128)(2,1)}) %all-gather.5.cloned.1.call-update) | async-done | bytes 2097168 | tf_op jit(solution)/shard_map/all_gather | solution.py:77
  322.6 3.0 slice_bitcast_fusion
  325.6 2.3 copy.26
  (29 shorter events, 0.1 us)
Async XLA Ops:
  7.2 1.9 copy-start
  7.2 193.6 %reduce-scatter.3.cloned.1.call-start = ((), (), s32[]{:S(2)}) async-start(), calls=%async_computation.2 | async-start | bytes 9437184 | tf_op jit(solution)/shard_map/reduce_scatter | solution.py:55
  9.1 3.2 copy-start.6
  9.1 3.3 copy-start.7
  9.1 5.2 %slice-start = ((s8[6291456]{0:T(1024)(128)(4,1)}), s8[4194304]{0:T(1024)(128)(4,1)S(1)}, s32[]{:S(2)}) async-start(s8[6291456]{0:T(1024)(128)(4,1)} %bitcast.52), calls=%async_computation.6 | async-start | bytes 8388608
  12.3 2.0 slice-start.1
  12.3 11.7 %slice-start.2 = ((s8[6291456]{0:T(1024)(128)(4,1)}), s8[4194304]{0:T(1024)(128)(4,1)S(1)}, s32[]{:S(2)}) async-start(s8[6291456]{0:T(1024)(128)(4,1)} %bitcast.54), calls=%async_computation.8 | async-start | bytes 8388608
  14.3 9.7 %slice-start.3 = ((s8[6291456]{0:T(1024)(128)(4,1)}), s8[2097152]{0:T(1024)(128)(4,1)S(1)}, s32[]{:S(2)}) async-start(s8[6291456]{0:T(1024)(128)(4,1)} %bitcast.54), calls=%async_computation.9 | async-start | bytes 4194304
  50.0 150.8 %copy-start.2 = (f32[2,256,128]{2,1,0:T(8,128)S(1)}, f32[2,256,128]{2,1,0:T(8,128)}, u32[]{:S(2)}) copy-start(f32[2,256,128]{2,1,0:T(8,128)} %param.16) | copy-start | bytes 786436
  50.0 151.0 %copy-start.3 = (f32[2,256,128]{2,1,0:T(8,128)S(1)}, f32[2,256,128]{2,1,0:T(8,128)}, u32[]{:S(2)}) copy-start(f32[2,256,128]{2,1,0:T(8,128)} %param.17) | copy-start | bytes 786436
  50.0 179.0 %copy-start.4 = (f32[256,256]{1,0:T(8,128)S(1)}, f32[256,256]{1,0:T(8,128)}, u32[]{:S(2)}) copy-start(f32[256,256]{1,0:T(8,128)} %param.14) | copy-start | bytes 786436
  50.1 177.2 %reduce-scatter.5.cloned.1.call-start = ((), (), s32[]{:S(2)}) async-start(), calls=%async_computation.3 | async-start | bytes 1310720 | tf_op jit(solution)/shard_map/reduce_scatter | solution.py:58
  200.8 70.4 %copy-start.5 = (f32[256,256]{1,0:T(8,128)S(1)}, f32[256,256]{1,0:T(8,128)}, u32[]{:S(2)}) copy-start(f32[256,256]{1,0:T(8,128)} %param.13) | copy-start | bytes 786436
  200.8 68.0 %all-gather.3.cloned.1.call-start = ((), (), s32[]{:S(2)}) async-start(), calls=%async_computation.4 | async-start | bytes 1310720 | tf_op jit(solution)/shard_map/all_gather | solution.py:67
  229.0 93.6 %all-gather.5.cloned.1.call-start = ((), (), s32[]{:S(2)}) async-start(), calls=%async_computation.5 | async-start | bytes 2359296 | tf_op jit(solution)/shard_map/all_gather | solution.py:77
  275.3 52.5 %copy-start.1 = (bf16[1536,1024]{1,0:T(8,128)(2,1)S(1)}, bf16[1536,1024]{1,0:T(8,128)(2,1)}, u32[]{:S(2)}) copy-start(bf16[1536,1024]{1,0:T(8,128)(2,1)} %param.10) | copy-start | bytes 9437188
Sparse Core Ops, SparseCore 0:
  50.2 150.5 reduce-scatter.2
  203.3 23.8 reduce-scatter.4
  229.4 16.7 all-gather.2
  272.9 49.6 all-gather.4
where the time goes:
time: 335 us; the launch traced here: 334 us
  waiting for transfers between devices  223 us (67%)
  blocking collectives  39.6 us (12%)
  matrix products  26.9 us (8%)
  other arithmetic  19.7 us (6%)
  between operations  14 us (4%)
  local copies, waits for them, and re-layouts  10.9 us (3%)
    reduce_scatter x1, waiting for transfers between devices, body(): lax.psum_scatter(jnp.stack((key_low, out_low), axis=1), 'fs', scatter_dim...  150 us
    all_gather x1, waiting for transfers between devices, body(): gathered = lax.all_gather(copies, 'fs', axis=1, tiled=True)  46.4 us
    psum x1, blocking collectives, body(): lax.psum(jnp.sum(direction * direction, axis=(1, 2)), ('fs', 'tp'))  39.6 us
    reduce_scatter x1, waiting for transfers between devices, body(): lax.psum_scatter(partial_low, 'tp', scatter_dimension=2, tiled=True)  26.1 us
    dot_general x2, matrix products, tokens_first(): lax.dot_general(left, right, (((0,), (0,)), ((), ())), preferred_element_...  19.4 us
    another operation x2, other arithmetic, body(): jnp.stack((key_low, out_low), axis=1)  16.3 us
    unnamed x32, local copies, waits for them, and re-layouts  7.89 us
  transfers between devices with their start and end apart: 4, of which 3 were waited for; matrix products, arithmetic and copies ran while one was open for 1% of the time, Pallas kernels for 0%

commit v1 on v0

v1 whole, which is shorter than its diff:
```python
import functools

import jax
import jax.numpy as jnp
from jax import lax
from jax.experimental import pallas as pl
from jax.experimental.pallas import tpu as pltpu
from jax.sharding import PartitionSpec as P

MESH = pl.DeviceIdType.MESH
f32 = jnp.float32
bf16 = jnp.bfloat16
first_decay = 0.8
second_decay = 0.9
learn_rate = 0.01


def kernel(
    fs, tp,
    x0_hbm, c0_hbm, c1_hbm, x1_hbm,
    key_w, out_w, bases, first_m, second_m,
    key_new, out_new, key_step, out_step, first_new, second_new, key_copy, out_copy,
    x_buf, c_buf, mapped, own, csnd, crcv, s2snd, s2rcv,
    y_own, y_snd, y_rcv, z0_snd, z0_rcv, z1_own, z1_snd, z1_rcv, x1_snd, x1_rcv,
    dirs, ss_snd, ss_rcv, tt_snd, tt_rcv,
    c_in, x_in, c_send, c_recv, s2_send, s2_recv, y_send, y_recv,
    z_send, z_recv, xx_send, xx_recv, d_send, d_recv, sst_send, sst_recv,
    ttt_send, ttt_recv, gz_send, gz_recv, gy_send, gy_recv,
):
    n = tp // 2
    nz = fs // n
    R, Q = first_m.shape[1], first_m.shape[2]
    W = key_w.shape[1]
    T = x_buf.shape[2]
    rank = bases.shape[2]
    half = rank // 2
    rows = n * R
    fi, ti = lax.axis_index("fs"), lax.axis_index("tp")
    core, xi = lax.rem(ti, 2), ti // 2
    zi, yi = fi // n, lax.rem(fi, n)

    def at_x(p):
        return (fi, p * 2 + core)

    def at_y(p):
        return (zi * n + p, ti)

    def at_z(p):
        return (p * n + yi, ti)

    def peer(me, d, size):
        return lax.rem(me + d, size)

    chunk = [peer(zi, 1 + i, nz) for i in range(nz)]
    loads = {}
    for m, (c_hbm, x_hbm) in ((1, (c1_hbm, x1_hbm)), (0, (c0_hbm, x0_hbm))):
        loads["c", m] = pltpu.make_async_copy(c_hbm, c_buf.at[m], c_in.at[m])
        for i in range(nz):
            cols = pl.ds(pl.multiple_of(chunk[i] * rows, 128), rows)
            loads[m, i] = pltpu.make_async_copy(x_hbm.at[:, cols], x_buf.at[m, i], x_in.at[m, i])
    items = [(m, i) for i in range(nz) for m in (1, 0)]
    loads["c", 1].start()
    loads[1, 0].start()
    loads["c", 0].start()
    for item in items[1:]:
        loads[item].start()

    sends = []

    def remote(src, dst, send, recv, where):
        copy = pltpu.make_async_remote_copy(
            src_ref=src, dst_ref=dst, send_sem=send, recv_sem=recv,
            device_id=where, device_id_type=MESH,
        )
        copy.start()
        sends.append(copy)
        return copy

    barrier = pltpu.get_barrier_semaphore()
    for d in range(1, tp):
        pl.semaphore_signal(barrier, inc=1, device_id=(fi, peer(ti, d, tp)), device_id_type=MESH)
    for d in range(1, fs):
        pl.semaphore_signal(barrier, inc=1, device_id=(peer(fi, d, fs), ti), device_id_type=MESH)

    def map_tokens(m):
        tile = T // 3 if T % 3 == 0 else T

        def step(k, carry):
            at = pl.ds(pl.multiple_of(k * tile, 128), tile)
            both = jnp.dot(c_buf[m, at, :], bases[m], preferred_element_type=f32)
            blocks = [both[:, t * Q:(t + 1) * Q] for t in range(tp)]
            pairs = [(blocks[2 * x], blocks[2 * x + 1]) for x in range(n)]
            kept = [jnp.where(core == 0, a, b) for a, b in pairs]
            sent = [jnp.where(core == 0, b, a) for a, b in pairs]
            mapped[m, at, :] = jnp.concatenate(kept + sent, axis=1).astype(bf16)
            return carry

        lax.fori_loop(0, T // tile, step, 0)

    def multiply(m, i):
        loads[m, i].wait()
        part = lax.dot_general(
            x_buf[m, i], mapped[m], (((0,), (0,)), ((), ())), preferred_element_type=f32
        )
        for x in range(n):
            for y in range(n):
                at = (x, y) if m == 0 else (y, x)
                block = part[y * R:(y + 1) * R]
                own[m, i, at[0], at[1]] = block[:, x * Q:(x + 1) * Q]
                csnd[m, i, at[0], at[1]] = block[:, half + x * Q:half + (x + 1) * Q].astype(bf16)

    flows = {}

    def second_stage(m, i):
        flows["c", m, i].wait_recv()
        total = own[m, i] + crcv[m, i].astype(f32)
        own[m, i] = total
        s2snd[m, i] = total.astype(bf16)
        for d in range(1, n):
            p = peer((xi, yi)[m], d, n)
            flows["s2", m, i, d] = remote(
                s2snd.at[m, i, p], s2rcv.at[m, i, d - 1],
                s2_send.at[m, i, d - 1], s2_recv.at[m, i, d - 1], (at_x, at_y)[m](p),
            )

    def third_stage(m, i):
        total = own[m, i, (xi, yi)[m]]
        for d in range(1, n):
            flows["s2", m, i, d].wait_recv()
            total = total + s2rcv[m, i, d - 1].astype(f32)
        if m == 1:
            if i == nz - 1:
                z1_own[...] = total
            else:
                z1_snd[i] = total.astype(bf16)
                flows["z", 1, i] = remote(
                    z1_snd.at[i], z1_rcv.at[i], z_send.at[1, i], z_recv.at[1, i], at_z(chunk[i])
                )
        else:
            y_own[i] = total
            y_snd[i] = total.astype(bf16)
            for d in range(1, n):
                p = peer(yi, d, n)
                flows["y", i, d] = remote(
                    y_snd.at[i, p], y_rcv.at[i, d - 1],
                    y_send.at[i, d - 1], y_recv.at[i, d - 1], at_y(p),
                )

    def fourth_stage(i):
        total = y_own[i, yi]
        for d in range(1, n):
            flows["y", i, d].wait_recv()
            total = total + y_rcv[i, d - 1].astype(f32)
        if i == nz - 1:
            return total
        z0_snd[i] = total.astype(bf16)
        flows["z", 0, i] = remote(
            z0_snd.at[i], z0_rcv.at[i], z_send.at[0, i], z_recv.at[0, i], at_z(chunk[i])
        )

    for k, (m, i) in enumerate(items):
        if i == 0:
            loads["c", m].wait()
            map_tokens(m)
        multiply(m, i)
        if k == 0:
            pl.semaphore_wait(barrier, tp + fs - 2)
        flows["c", m, i] = remote(
            csnd.at[m, i], crcv.at[m, i], c_send.at[m, i], c_recv.at[m, i],
            (fi, xi * 2 + 1 - core),
        )
        if k >= 1:
            second_stage(*items[k - 1])
        if k >= 3:
            third_stage(*items[k - 3])
        if k >= 5 and items[k - 5][0] == 0:
            fourth_stage(items[k - 5][1])
    last = len(items)
    second_stage(*items[last - 1])
    third_stage(*items[last - 3])
    if items[last - 5][0] == 0:
        fourth_stage(items[last - 5][1])
    third_stage(*items[last - 2])
    third_stage(*items[last - 1])
    total0 = None
    for i in range(nz):
        if ("z", 0, i) not in flows:
            total0 = fourth_stage(i)

    total1 = z1_own[...]
    for i in range(nz - 1):
        flows["z", 1, i].wait_recv()
        total1 = total1 + z1_rcv[i].astype(f32)
    z1_own[...] = total1
    x1_snd[...] = total1.astype(bf16)
    for d in range(1, n):
        p = peer(xi, d, n)
        flows["x", d] = remote(
            x1_snd.at[p], x1_rcv.at[d - 1], xx_send.at[d - 1], xx_recv.at[d - 1], at_x(p)
        )

    def update(m, reduced):
        first = first_decay * first_m[m] + (1.0 - first_decay) * reduced
        second = second_decay * second_m[m] + (1.0 - second_decay) * reduced * reduced
        direction = first / jnp.sqrt(second)
        first_new[m] = first
        second_new[m] = second
        dirs[m, ti] = direction.astype(bf16)
        for d in range(1, tp):
            flows["d", m, d] = remote(
                dirs.at[m, ti], dirs.at[m, ti], d_send.at[m, d - 1], d_recv.at[m, d - 1],
                (fi, peer(ti, d, tp)),
            )
        return jnp.sum(direction * direction, keepdims=True)

    for i in range(nz - 1):
        flows["z", 0, i].wait_recv()
        total0 = total0 + z0_rcv[i].astype(f32)
    sum0 = update(0, total0)
    reduced1 = z1_own[xi]
    for d in range(1, n):
        flows["x", d].wait_recv()
        reduced1 = reduced1 + x1_rcv[d - 1].astype(f32)
    sum1 = update(1, reduced1)

    line = lax.broadcasted_iota(jnp.int32, ss_snd.shape, 0)
    squares = jnp.where(line == 0, sum0, sum1)
    ss_snd[...] = squares
    for d in range(1, tp):
        flows["ss", d] = remote(
            ss_snd, ss_rcv.at[d - 1], sst_send.at[d - 1], sst_recv.at[d - 1],
            (fi, peer(ti, d, tp)),
        )
    for d in range(1, tp):
        flows["ss", d].wait_recv()
        squares = squares + ss_rcv[d - 1]
    tt_snd[...] = squares
    for d in range(1, fs):
        flows["tt", d] = remote(
            tt_snd, tt_rcv.at[d - 1], ttt_send.at[d - 1], ttt_recv.at[d - 1],
            (peer(fi, d, fs), ti),
        )
    local = pl.ds(pl.multiple_of(ti * W, 128), W)
    projected = []
    for m in range(2):
        for d in range(1, tp):
            flows["d", m, d].wait_recv()
        whole = jnp.concatenate([dirs[m, t] for t in range(tp)], axis=1)
        base = bases[m, local, :]
        left, right = ((whole, base), (base, whole))[m]
        projected.append(
            lax.dot_general(left, right, (((1,), (1,)), ((), ())), preferred_element_type=f32)
        )
    for d in range(1, fs):
        flows["tt", d].wait_recv()
        squares = squares + tt_rcv[d - 1]
    scales = lax.rsqrt(squares / (fs * R * rank) + 1.0)

    def key_at(f):
        return key_copy.at[pl.ds(pl.multiple_of(f * R, 128), R), :]

    def out_at(f):
        return out_copy.at[:, pl.ds(pl.multiple_of(f * R, 128), R)]

    pieces = (key_at, out_at)

    def to_y(slot, f, m):
        for d in range(1, n):
            flows["gy", slot, d, m] = remote(
                pieces[m](f), pieces[m](f), gy_send.at[slot, d - 1, m], gy_recv.at[slot, d - 1, m],
                at_y(peer(yi, d, n)),
            )

    for m, (step_ref, new_ref, weight) in enumerate(
        ((key_step, key_new, key_w), (out_step, out_new, out_w))
    ):
        step = projected[m] * scales[m:m + 1, 0:1]
        new = weight[...] - learn_rate * step
        step_ref[...] = step
        new_ref[...] = new
        pieces[m](fi)[...] = new.astype(bf16)
        to_y(nz - 1, fi, m)
        for d in range(1, nz):
            flows["gz", d, m] = remote(
                pieces[m](fi), pieces[m](fi), gz_send.at[d - 1, m], gz_recv.at[d - 1, m],
                at_z(peer(zi, d, nz)),
            )
    for d in range(1, nz):
        for m in range(2):
            flows["gz", d, m].wait_recv()
            to_y(d - 1, peer(zi, nz - d, nz) * n + yi, m)
    for slot in range(nz):
        for d in range(1, n):
            for m in range(2):
                flows["gy", slot, d, m].wait_recv()
    for copy in sends:
        copy.wait_send()


def solution(mesh):
    fs, tp = mesh.shape["fs"], mesh.shape["tp"]
    n = tp // 2
    nz = fs // n

    def body(saved_input, key_cot, mixed_out, out_cot, key_weight, out_weight, bases, first_moment, second_moment):
        R, Q = first_moment.shape[1:]
        T, D = saved_input.shape
        K = key_cot.shape[1]
        rank = bases.shape[2]
        rows = n * R
        vmem = pl.BlockSpec(memory_space=pltpu.VMEM)
        hbm = pl.BlockSpec(memory_space=pltpu.HBM)
        dma = pltpu.SemaphoreType.DMA

        def shape(a):
            return jax.ShapeDtypeStruct(a.shape, f32)

        W = key_weight.shape[1]
        outs = (
            shape(key_weight), shape(out_weight), shape(key_weight), shape(out_weight),
            shape(first_moment), shape(second_moment),
            jax.ShapeDtypeStruct((D, W), bf16), jax.ShapeDtypeStruct((W, D), bf16),
        )
        V = pltpu.VMEM
        o = max(n - 1, 1)
        scratch = [
            V((2, nz, T, rows), bf16), V((2, T, K), bf16), V((2, T, rank), bf16),
            V((2, nz, n, n, R, Q), f32), V((2, nz, n, n, R, Q), bf16), V((2, nz, n, n, R, Q), bf16),
            V((2, nz, n, n, R, Q), bf16), V((2, nz, o, n, R, Q), bf16),
            V((nz, n, R, Q), f32), V((nz, n, R, Q), bf16), V((nz, o, R, Q), bf16),
            V((nz - 1, R, Q), bf16), V((nz - 1, R, Q), bf16),
            V((n, R, Q), f32), V((nz - 1, n, R, Q), bf16), V((nz - 1, n, R, Q), bf16),
            V((n, R, Q), bf16), V((o, R, Q), bf16),
            V((2, tp, R, Q), bf16),
            V((8, 128), f32), V((tp - 1, 8, 128), f32), V((8, 128), f32), V((fs - 1, 8, 128), f32),
            dma((2,)), dma((2, nz)), dma((2, nz)), dma((2, nz)),
            dma((2, nz, o)), dma((2, nz, o)), dma((nz, o)), dma((nz, o)),
            dma((2, nz - 1)), dma((2, nz - 1)), dma((o,)), dma((o,)),
            dma((2, tp - 1)), dma((2, tp - 1)), dma((tp - 1,)), dma((tp - 1,)),
            dma((fs - 1,)), dma((fs - 1,)), dma((nz - 1, 2)), dma((nz - 1, 2)),
            dma((nz, o, 2)), dma((nz, o, 2)),
        ]
        return pl.pallas_call(
            functools.partial(kernel, fs, tp),
            out_shape=outs,
            in_specs=[hbm] * 4 + [vmem] * 5,
            out_specs=[vmem] * 8,
            scratch_shapes=scratch,
            compiler_params=pltpu.CompilerParams(
                collective_id=0, has_side_effects=True, vmem_limit_bytes=60 * 1024 * 1024
            ),
        )(saved_input, key_cot, mixed_out, out_cot, key_weight, out_weight, bases, first_moment, second_moment)

    rows_placed = P(("fs", "tp"), None)
    return jax.shard_map(
        body,
        mesh=mesh,
        in_specs=(rows_placed,) * 4
        + (P("fs", "tp"), P("tp", "fs"), P(), P(None, "fs", "tp"), P(None, "fs", "tp")),
        out_specs=(
            P("fs", "tp"), P("tp", "fs"), P("fs", "tp"), P("tp", "fs"),
            P(None, "fs", "tp"), P(None, "fs", "tp"), P(None, "tp"), P("tp", None),
        ),
        check_vma=False,
    )
```

time: 335 us -> 99.6 us (0.30)
  the two profiles are of different devices: /device:TPU:0 before, /device:TPU:16 now
where the time goes in v1:
time: 99.6 us; the launch traced here: 99.2 us
  Pallas kernels  86.5 us (87%)
  local copies, waits for them, and re-layouts  12.1 us (12%)
    pallas_call x1, Pallas kernels, body(): pl.pallas_call(functools.partial(kernel, fs, tp), out_shape=outs, in_spec...  86.5 us
    unnamed x12, local copies, waits for them, and re-layouts  12.1 us

profile of v1, /device:TPU:16, one launch (start us, length us, event | category | flops | bytes accessed | tf_op | source)
XLA Modules:
  0.0 99.2 jit_solution(17385622388657165187)
XLA Ops:
  0.6 86.5 %shard_map.152 = (f32[256,256]{1,0:T(8,128)}, f32[256,256]{1,0:T(8,128)}, f32[256,256]{1,0:T(8,128)}, f32[256,256]{1,0:T(8,128)}, f32[2,256,128]{2,1,0:T(8,128)}...) custom-call(bf16[1536,2048]{1,0:T(8,128)(2,1)} %x0_hbm.1, ...), custom_call_target="tpu_custom_call" | custom-call | tf_op jit(solution)/shard_map/pallas_call | solution.py:343
  87.1 0.0 copy-start.1
  87.1 0.0 copy-start
  87.1 1.8 %copy.25 = f32[256,256]{1,0:T(8,128)} copy(f32[256,256]{1,0:T(8,128)} %get-tuple-element.16) | data formatting | bytes 524288
  89.0 1.7 %copy.26 = f32[256,256]{1,0:T(8,128)} copy(f32[256,256]{1,0:T(8,128)} %get-tuple-element.17) | data formatting | bytes 524288
  90.6 1.7 %copy.27 = f32[256,256]{1,0:T(8,128)} copy(f32[256,256]{1,0:T(8,128)} %get-tuple-element.18) | data formatting | bytes 524288
  92.3 1.7 %copy.28 = f32[256,256]{1,0:T(8,128)} copy(f32[256,256]{1,0:T(8,128)} %get-tuple-element.19) | data formatting | bytes 524288
  94.0 1.7 %copy.29 = f32[2,256,128]{2,1,0:T(8,128)} copy(f32[2,256,128]{2,1,0:T(8,128)} %get-tuple-element.20) | data formatting | bytes 524288
  95.6 1.7 %copy.30 = f32[2,256,128]{2,1,0:T(8,128)} copy(f32[2,256,128]{2,1,0:T(8,128)} %get-tuple-element.21) | data formatting | bytes 524288
  97.3 0.0 copy-done.1
  97.3 1.0 copy.31
  98.3 0.0 copy-done
  98.3 1.0 copy.32
Async XLA Ops:
  87.1 10.2 %copy-start.1 = (bf16[2048,256]{1,0:T(8,128)(2,1)S(1)}, bf16[2048,256]{1,0:T(8,128)(2,1)}, u32[]{:S(2)}) copy-start(bf16[2048,256]{1,0:T(8,128)(2,1)} %get-tuple-element.22) | copy-start | bytes 3145732
  87.1 11.1 %copy-start = (bf16[256,2048]{1,0:T(8,128)(2,1)S(1)}, bf16[256,2048]{1,0:T(8,128)(2,1)}, u32[]{:S(2)}) copy-start(bf16[256,2048]{1,0:T(8,128)(2,1)} %get-tuple-element.23) | copy-start | bytes 3145732

commit v2 on v1

v2 whole, which is shorter than its diff:
```python
import functools

import jax
import jax.numpy as jnp
from jax import lax
from jax.experimental import pallas as pl
from jax.experimental.pallas import tpu as pltpu
from jax.sharding import PartitionSpec as P

MESH = pl.DeviceIdType.MESH
f32 = jnp.float32
bf16 = jnp.bfloat16
first_decay = 0.8
second_decay = 0.9
learn_rate = 0.01


def kernel(
    fs, tp,
    x0_hbm, c0_hbm, c1_hbm, x1_hbm,
    key_w_hbm, out_w_hbm, bases_hbm, first_hbm, second_hbm,
    key_new, out_new, key_step, out_step, first_new, second_new, key_copy, out_copy,
    key_w, out_w, bases, first_m, second_m, x_buf, c_buf, mapped, own, csnd, crcv, s2snd, s2rcv,
    y_own, y_snd, y_rcv, z0_snd, z0_rcv, z1_own, z1_snd, z1_rcv, x1_snd, x1_rcv,
    dirs, ss_snd, ss_rcv, tt_snd, tt_rcv,
    b_in, w_in, c_in, x_in, c_send, c_recv, s2_send, s2_recv, y_send, y_recv,
    z_send, z_recv, xx_send, xx_recv, d_send, d_recv, sst_send, sst_recv,
    ttt_send, ttt_recv, gz_send, gz_recv, gy_send, gy_recv,
):
    n = tp // 2
    nz = fs // n
    R, Q = first_m.shape[1], first_m.shape[2]
    W = key_w.shape[1]
    T = x_buf.shape[2]
    rank = bases.shape[2]
    half = rank // 2
    rows = n * R
    fi, ti = lax.axis_index("fs"), lax.axis_index("tp")
    core, xi = lax.rem(ti, 2), ti // 2
    zi, yi = fi // n, lax.rem(fi, n)

    def at_x(p):
        return (fi, p * 2 + core)

    def at_y(p):
        return (zi * n + p, ti)

    def at_z(p):
        return (p * n + yi, ti)

    def peer(me, d, size):
        return lax.rem(me + d, size)

    chunk = [peer(zi, 1 + i, nz) for i in range(nz)]
    tiles = 3 if T % 3 == 0 else 1
    tile = T // tiles
    loads = {}
    for m, (c_hbm, x_hbm) in ((1, (c1_hbm, x1_hbm)), (0, (c0_hbm, x0_hbm))):
        loads["b", m] = pltpu.make_async_copy(bases_hbm.at[m], bases.at[m], b_in.at[m])
        for k in range(tiles):
            at = pl.ds(k * tile, tile)
            loads["c", m, k] = pltpu.make_async_copy(c_hbm.at[at], c_buf.at[m, at], c_in.at[m, k])
        for i in range(nz):
            cols = pl.ds(pl.multiple_of(chunk[i] * rows, 128), rows)
            loads[m, i] = pltpu.make_async_copy(x_hbm.at[:, cols], x_buf.at[m, i], x_in.at[m, i])
    rest = (
        (first_hbm, first_m), (second_hbm, second_m), (key_w_hbm, key_w), (out_w_hbm, out_w)
    )
    for k, (source, target) in enumerate(rest):
        loads["w", k] = pltpu.make_async_copy(source, target, w_in.at[k])
    items = [(m, i) for m in (1, 0) for i in range(nz)]
    for copy in loads.values():
        copy.start()

    sends = []

    def remote(src, dst, send, recv, where):
        copy = pltpu.make_async_remote_copy(
            src_ref=src, dst_ref=dst, send_sem=send, recv_sem=recv,
            device_id=where, device_id_type=MESH,
        )
        copy.start()
        sends.append(copy)
        return copy

    barrier = pltpu.get_barrier_semaphore()
    for d in range(1, tp):
        pl.semaphore_signal(barrier, inc=1, device_id=(fi, peer(ti, d, tp)), device_id_type=MESH)
    for d in range(1, fs):
        pl.semaphore_signal(barrier, inc=1, device_id=(peer(fi, d, fs), ti), device_id_type=MESH)

    def map_tokens(m):
        loads["b", m].wait()
        for k in range(tiles):
            loads["c", m, k].wait()
            at = pl.ds(k * tile, tile)
            both = jnp.dot(c_buf[m, at, :], bases[m], preferred_element_type=f32)
            blocks = [both[:, t * Q:(t + 1) * Q] for t in range(tp)]
            pairs = [(blocks[2 * x], blocks[2 * x + 1]) for x in range(n)]
            kept = [jnp.where(core == 0, a, b) for a, b in pairs]
            sent = [jnp.where(core == 0, b, a) for a, b in pairs]
            mapped[m, at, :] = jnp.concatenate(kept + sent, axis=1).astype(bf16)

    def multiply(m, i):
        loads[m, i].wait()
        part = lax.dot_general(
            x_buf[m, i], mapped[m], (((0,), (0,)), ((), ())), preferred_element_type=f32
        )
        for x in range(n):
            for y in range(n):
                at = (x, y) if m == 0 else (y, x)
                block = part[y * R:(y + 1) * R]
                own[m, i, at[0], at[1]] = block[:, x * Q:(x + 1) * Q]
                csnd[m, i, at[0], at[1]] = block[:, half + x * Q:half + (x + 1) * Q].astype(bf16)

    flows = {}

    def second_stage(m, i):
        flows["c", m, i].wait_recv()
        total = own[m, i] + crcv[m, i].astype(f32)
        own[m, i] = total
        s2snd[m, i] = total.astype(bf16)
        for d in range(1, n):
            p = peer((xi, yi)[m], d, n)
            flows["s2", m, i, d] = remote(
                s2snd.at[m, i, p], s2rcv.at[m, i, d - 1],
                s2_send.at[m, i, d - 1], s2_recv.at[m, i, d - 1], (at_x, at_y)[m](p),
            )

    def third_stage(m, i):
        total = own[m, i, (xi, yi)[m]]
        for d in range(1, n):
            flows["s2", m, i, d].wait_recv()
            total = total + s2rcv[m, i, d - 1].astype(f32)
        if m == 1:
            if i == nz - 1:
                z1_own[...] = total
            else:
                z1_snd[i] = total.astype(bf16)
                flows["z", 1, i] = remote(
                    z1_snd.at[i], z1_rcv.at[i], z_send.at[1, i], z_recv.at[1, i], at_z(chunk[i])
                )
        else:
            y_own[i] = total
            y_snd[i] = total.astype(bf16)
            for d in range(1, n):
                p = peer(yi, d, n)
                flows["y", i, d] = remote(
                    y_snd.at[i, p], y_rcv.at[i, d - 1],
                    y_send.at[i, d - 1], y_recv.at[i, d - 1], at_y(p),
                )

    def fourth_stage(i):
        total = y_own[i, yi]
        for d in range(1, n):
            flows["y", i, d].wait_recv()
            total = total + y_rcv[i, d - 1].astype(f32)
        if i == nz - 1:
            return total
        z0_snd[i] = total.astype(bf16)
        flows["z", 0, i] = remote(
            z0_snd.at[i], z0_rcv.at[i], z_send.at[0, i], z_recv.at[0, i], at_z(chunk[i])
        )

    def sum_z1():
        total = z1_own[...]
        for i in range(nz - 1):
            flows["z", 1, i].wait_recv()
            total = total + z1_rcv[i].astype(f32)
        z1_own[...] = total
        x1_snd[...] = total.astype(bf16)
        for d in range(1, n):
            p = peer(xi, d, n)
            flows["x", d] = remote(
                x1_snd.at[p], x1_rcv.at[d - 1], xx_send.at[d - 1], xx_recv.at[d - 1], at_x(p)
            )

    def sum_x1():
        total = z1_own[xi]
        for d in range(1, n):
            flows["x", d].wait_recv()
            total = total + x1_rcv[d - 1].astype(f32)
        return total

    def sum_z0(total):
        for i in range(nz - 1):
            flows["z", 0, i].wait_recv()
            total = total + z0_rcv[i].astype(f32)
        return total

    def update(m, reduced):
        first = first_decay * first_m[m] + (1.0 - first_decay) * reduced
        second = second_decay * second_m[m] + (1.0 - second_decay) * reduced * reduced
        direction = first / jnp.sqrt(second)
        squares = jnp.broadcast_to(jnp.sum(direction * direction, keepdims=True), (8, 128))
        ss_snd[m] = squares
        dirs[m, ti] = direction.astype(bf16)
        for d in range(1, tp):
            where = (fi, peer(ti, d, tp))
            flows["ss", m, d] = remote(
                ss_snd.at[m], ss_rcv.at[m, d - 1], sst_send.at[m, d - 1], sst_recv.at[m, d - 1], where
            )
            flows["d", m, d] = remote(
                dirs.at[m, ti], dirs.at[m, ti], d_send.at[m, d - 1], d_recv.at[m, d - 1], where
            )
        first_new[m] = first
        second_new[m] = second

    def sum_tp(m):
        squares = ss_snd[m]
        for d in range(1, tp):
            flows["ss", m, d].wait_recv()
            squares = squares + ss_rcv[m, d - 1]
        tt_snd[m] = squares
        for d in range(1, fs):
            flows["tt", m, d] = remote(
                tt_snd.at[m], tt_rcv.at[m, d - 1], ttt_send.at[m, d - 1], ttt_recv.at[m, d - 1],
                (peer(fi, d, fs), ti),
            )

    def project(m):
        for d in range(1, tp):
            flows["d", m, d].wait_recv()
        whole = jnp.concatenate([dirs[m, t] for t in range(tp)], axis=1)
        base = bases[m, pl.ds(pl.multiple_of(ti * W, 128), W), :]
        left, right = ((whole, base), (base, whole))[m]
        (key_step, out_step)[m][...] = lax.dot_general(
            left, right, (((1,), (1,)), ((), ())), preferred_element_type=f32
        )

    def key_at(z, y):
        return key_copy.at[pl.ds(pl.multiple_of((z * n + y) * R, 128), R), :]

    def out_at(z, y):
        return out_copy.at[:, pl.ds(pl.multiple_of((z * n + y) * R, 128), R)]

    pieces = (key_at, out_at)

    def line_copy(m, up, hop):
        piece = pieces[m](zi - hop if up else zi + hop, yi)
        side = 0 if up else 1
        return pltpu.make_async_remote_copy(
            src_ref=piece, dst_ref=piece, send_sem=gz_send.at[m, side, hop], recv_sem=gz_recv.at[m, side, hop],
            device_id=at_z(zi + 1 if up else zi - 1), device_id_type=MESH,
        )

    def may_send(up, hop):
        if up:
            return (zi >= hop) & (zi < nz - 1)
        return (zi + hop < nz) & (zi > 0)

    def side_copies(m, z):
        piece = pieces[m](z, yi)
        return [
            pltpu.make_async_remote_copy(
                src_ref=piece, dst_ref=piece, send_sem=gy_send.at[m, z, d - 1], recv_sem=gy_recv.at[m, z, d - 1],
                device_id=at_y(peer(yi, d, n)), device_id_type=MESH,
            )
            for d in range(1, n)
        ]

    def start_line(m, up, hop):
        @pl.when(may_send(up, hop))
        def _():
            line_copy(m, up, hop).start()

    def finish(m):
        squares = tt_snd[m]
        for d in range(1, fs):
            flows["tt", m, d].wait_recv()
            squares = squares + tt_rcv[m, d - 1]
        scale = lax.rsqrt(squares / (fs * R * rank) + 1.0)[0:1, 0:1]
        step_ref, new_ref, weight = ((key_step, key_new, key_w), (out_step, out_new, out_w))[m]
        step = step_ref[...] * scale
        new = weight[...] - learn_rate * step
        pieces[m](zi, yi)[...] = new.astype(bf16)
        for up in (True, False):
            start_line(m, up, 0)
        for copy in side_copies(m, zi):
            copy.start()
        step_ref[...] = step
        new_ref[...] = new

    def relay(m, hop):
        for up in (True, False):
            @pl.when((zi >= hop) if up else (zi + hop < nz))
            def _():
                line_copy(m, up, hop - 1).wait_recv()
                if hop < nz - 1:
                    start_line(m, up, hop)
                for copy in side_copies(m, zi - hop if up else zi + hop):
                    copy.start()

    def close(m):
        for z in range(nz):
            for copy in side_copies(m, z):
                copy.wait_recv()
        for z in range(nz):
            for copy in side_copies(m, z):
                copy.wait_send()
        for hop in range(nz - 1):
            for up in (True, False):
                @pl.when(may_send(up, hop))
                def _():
                    line_copy(m, up, hop).wait_send()

    for k, (m, i) in enumerate(items):
        if i == 0:
            map_tokens(m)
        multiply(m, i)
        if k == 0:
            pl.semaphore_wait(barrier, tp + fs - 2)
        flows["c", m, i] = remote(
            csnd.at[m, i], crcv.at[m, i], c_send.at[m, i], c_recv.at[m, i],
            (fi, xi * 2 + 1 - core),
        )
        if k >= 1:
            second_stage(*items[k - 1])
        if k >= 3:
            third_stage(*items[k - 3])
    second_stage(0, nz - 1)
    for k in range(len(rest)):
        loads["w", k].wait()
    for k in range(len(items) - 3, len(items)):
        if items[k][0] == 1:
            third_stage(*items[k])
    waiting = [items[k][1] for k in range(len(items) - 3, len(items)) if items[k][0] == 0]
    third_stage(0, waiting[0])
    sum_z1()
    for i in waiting[1:]:
        third_stage(0, i)
    for i in range(nz - 2):
        fourth_stage(i)
    update(1, sum_x1())
    fourth_stage(nz - 2)
    total0 = fourth_stage(nz - 1)
    sum_tp(1)
    project(1)
    update(0, sum_z0(total0))
    finish(1)
    sum_tp(0)
    relay(1, 1)
    project(0)
    finish(0)
    for hop in range(2, nz):
        relay(1, hop)
        relay(0, hop - 1)
    relay(0, nz - 1)
    close(1)
    close(0)
    for copy in sends:
        copy.wait_send()


def move_out(*refs):
    count = len(refs) // 2
    copies = [
        pltpu.make_async_copy(refs[k], refs[count + k], refs[-1].at[k]) for k in range(count)
    ]
    for copy in copies:
        copy.start()
    for copy in copies:
        copy.wait()


def solution(mesh):
    fs, tp = mesh.shape["fs"], mesh.shape["tp"]
    n = tp // 2
    nz = fs // n

    def body(saved_input, key_cot, mixed_out, out_cot, key_weight, out_weight, bases, first_moment, second_moment):
        R, Q = first_moment.shape[1:]
        T, D = saved_input.shape
        K = key_cot.shape[1]
        rank = bases.shape[2]
        rows = n * R
        vmem = pl.BlockSpec(memory_space=pltpu.VMEM)
        hbm = pl.BlockSpec(memory_space=pltpu.HBM)
        dma = pltpu.SemaphoreType.DMA

        def shape(a):
            return jax.ShapeDtypeStruct(a.shape, f32)

        W = key_weight.shape[1]
        outs = (
            shape(key_weight), shape(out_weight), shape(key_weight), shape(out_weight),
            shape(first_moment), shape(second_moment),
            jax.ShapeDtypeStruct((D, W), bf16), jax.ShapeDtypeStruct((W, D), bf16),
        )
        V = pltpu.VMEM
        o = max(n - 1, 1)
        scratch = [
            V((R, W), f32), V((W, R), f32), V(bases.shape, bf16), V((2, R, Q), f32), V((2, R, Q), f32),
            V((2, nz, T, rows), bf16), V((2, T, K), bf16), V((2, T, rank), bf16),
            V((2, nz, n, n, R, Q), f32), V((2, nz, n, n, R, Q), bf16), V((2, nz, n, n, R, Q), bf16),
            V((2, nz, n, n, R, Q), bf16), V((2, nz, o, n, R, Q), bf16),
            V((nz, n, R, Q), f32), V((nz, n, R, Q), bf16), V((nz, o, R, Q), bf16),
            V((nz - 1, R, Q), bf16), V((nz - 1, R, Q), bf16),
            V((n, R, Q), f32), V((nz - 1, n, R, Q), bf16), V((nz - 1, n, R, Q), bf16),
            V((n, R, Q), bf16), V((o, R, Q), bf16),
            V((2, tp, R, Q), bf16),
            V((2, 8, 128), f32), V((2, tp - 1, 8, 128), f32), V((2, 8, 128), f32), V((2, fs - 1, 8, 128), f32),
            dma((2,)), dma((4,)), dma((2, 3)), dma((2, nz)), dma((2, nz)), dma((2, nz)),
            dma((2, nz, o)), dma((2, nz, o)), dma((nz, o)), dma((nz, o)),
            dma((2, nz - 1)), dma((2, nz - 1)), dma((o,)), dma((o,)),
            dma((2, tp - 1)), dma((2, tp - 1)), dma((2, tp - 1)), dma((2, tp - 1)),
            dma((2, fs - 1)), dma((2, fs - 1)), dma((2, 2, nz - 1)), dma((2, 2, nz - 1)),
            dma((2, nz, o)), dma((2, nz, o)),
        ]
        results = pl.pallas_call(
            functools.partial(kernel, fs, tp),
            out_shape=outs,
            in_specs=[hbm] * 9,
            out_specs=[vmem] * 8,
            scratch_shapes=scratch,
            compiler_params=pltpu.CompilerParams(
                collective_id=0, has_side_effects=True, vmem_limit_bytes=54 * 1024 * 1024
            ),
        )(saved_input, key_cot, mixed_out, out_cot, key_weight, out_weight, bases, first_moment, second_moment)
        return pl.pallas_call(
            move_out,
            out_shape=outs,
            in_specs=[pl.BlockSpec(memory_space=pl.ANY)] * 8,
            out_specs=[hbm] * 8,
            scratch_shapes=[dma((8,))],
            compiler_params=pltpu.CompilerParams(vmem_limit_bytes=1024 * 1024),
        )(*results)

    rows_placed = P(("fs", "tp"), None)
    return jax.shard_map(
        body,
        mesh=mesh,
        in_specs=(rows_placed,) * 4
        + (P("fs", "tp"), P("tp", "fs"), P(), P(None, "fs", "tp"), P(None, "fs", "tp")),
        out_specs=(
            P("fs", "tp"), P("tp", "fs"), P("fs", "tp"), P("tp", "fs"),
            P(None, "fs", "tp"), P(None, "fs", "tp"), P(None, "tp"), P("tp", None),
        ),
        check_vma=False,
    )
```

time: 99.6 us -> 85.5 us (0.86)
  the two profiles are of different devices: /device:TPU:16 before, /device:TPU:0 now
where the time goes in v2:
time: 85.5 us; the launch traced here: 85.1 us
  Pallas kernels  76.3 us (89%)
  local copies, waits for them, and re-layouts  8.14 us (10%)
    pallas_call x1, Pallas kernels, body(): pl.pallas_call(functools.partial(kernel, fs, tp), out_shape=outs, in_spec...  74.4 us
    unnamed x16, local copies, waits for them, and re-layouts  8.14 us
    pallas_call x1, Pallas kernels, body(): pl.pallas_call(move_out, out_shape=outs, in_specs=[pl.BlockSpec(memory_sp...  1.9 us

profile of v2, /device:TPU:0, one launch (start us, length us, event | category | flops | bytes accessed | tf_op | source)
XLA Modules:
  0.0 85.1 jit_solution(14144517809474077098)
XLA Ops:
  0.6 74.4 %shard_map.152 = (f32[256,256]{1,0:T(8,128)}, f32[256,256]{1,0:T(8,128)}, f32[256,256]{1,0:T(8,128)}, f32[256,256]{1,0:T(8,128)}, f32[2,256,128]{2,1,0:T(8,128)}...) custom-call(bf16[1536,2048]{1,0:T(8,128)(2,1)} %x0_hbm.1, ...), custom_call_target="tpu_custom_call" | custom-call | tf_op jit(solution)/shard_map/pallas_call | solution.py:410
  75.0 0.0 copy-start
  75.0 1.2 %copy-done = bf16[2048,256]{1,0:T(8,128)(2,1)S(1)} copy-done((bf16[2048,256]{1,0:T(8,128)(2,1)S(1)}, bf16[2048,256]{1,0:T(8,128)(2,1)}, u32[]{:S(2)}) %copy-start) | copy-done | bytes 1048600
  76.3 0.0 copy-start.1
  76.3 1.2 %copy-done.1 = bf16[256,2048]{1,0:T(8,128)(2,1)S(1)} copy-done((bf16[256,2048]{1,0:T(8,128)(2,1)S(1)}, bf16[256,2048]{1,0:T(8,128)(2,1)}, u32[]{:S(2)}) %copy-start.1) | copy-done | bytes 1048600
  77.5 0.0 copy-start.2
  77.5 0.9 %copy-done.2 = f32[256,256]{1,0:T(8,128)S(1)} copy-done((f32[256,256]{1,0:T(8,128)S(1)}, f32[256,256]{1,0:T(8,128)}, u32[]{:S(2)}) %copy-start.2) | copy-done | bytes 262168
  78.4 0.0 copy-start.3
  78.4 0.9 %copy-done.3 = f32[256,256]{1,0:T(8,128)S(1)} copy-done((f32[256,256]{1,0:T(8,128)S(1)}, f32[256,256]{1,0:T(8,128)}, u32[]{:S(2)}) %copy-start.3) | copy-done | bytes 262168
  79.4 0.0 copy-start.4
  79.4 0.9 %copy-done.4 = f32[256,256]{1,0:T(8,128)S(1)} copy-done((f32[256,256]{1,0:T(8,128)S(1)}, f32[256,256]{1,0:T(8,128)}, u32[]{:S(2)}) %copy-start.4) | copy-done | bytes 262168
  80.3 0.0 copy-start.5
  80.3 0.9 %copy-done.5 = f32[256,256]{1,0:T(8,128)S(1)} copy-done((f32[256,256]{1,0:T(8,128)S(1)}, f32[256,256]{1,0:T(8,128)}, u32[]{:S(2)}) %copy-start.5) | copy-done | bytes 262168
  81.3 0.0 copy-start.6
  81.3 0.9 %copy-done.6 = f32[2,256,128]{2,1,0:T(8,128)S(1)} copy-done((f32[2,256,128]{2,1,0:T(8,128)S(1)}, f32[2,256,128]{2,1,0:T(8,128)}, u32[]{:S(2)}) %copy-start.6) | copy-done | bytes 262168
  82.2 0.0 copy-start.7
  82.2 0.9 %copy-done.7 = f32[2,256,128]{2,1,0:T(8,128)S(1)} copy-done((f32[2,256,128]{2,1,0:T(8,128)S(1)}, f32[2,256,128]{2,1,0:T(8,128)}, u32[]{:S(2)}) %copy-start.7) | copy-done | bytes 262168
  83.2 1.9 %shard_map.153 = (f32[256,256]{1,0:T(8,128)}, f32[256,256]{1,0:T(8,128)}, f32[256,256]{1,0:T(8,128)}, f32[256,256]{1,0:T(8,128)}, f32[2,256,128]{2,1,0:T(8,128)}...) custom-call(f32[256,256]{1,0:T(8,128)S(1)} %copy-done.2, f32[256,256]{1,0:T(8,128)S(1)} %copy-done.3, ...), custom_call_target="tpu_custom_call" | custom-call | tf_op jit(solution)/shard_map/pallas_call | solution.py:420
Async XLA Ops:
  75.0 1.2 %copy-start = (bf16[2048,256]{1,0:T(8,128)(2,1)S(1)}, bf16[2048,256]{1,0:T(8,128)(2,1)}, u32[]{:S(2)}) copy-start(bf16[2048,256]{1,0:T(8,128)(2,1)} %get-tuple-element.22.refs_6_) | copy-start | bytes 3145732
  76.3 1.2 %copy-start.1 = (bf16[256,2048]{1,0:T(8,128)(2,1)S(1)}, bf16[256,2048]{1,0:T(8,128)(2,1)}, u32[]{:S(2)}) copy-start(bf16[256,2048]{1,0:T(8,128)(2,1)} %get-tuple-element.23.refs_7_) | copy-start | bytes 3145732
  77.5 0.9 %copy-start.2 = (f32[256,256]{1,0:T(8,128)S(1)}, f32[256,256]{1,0:T(8,128)}, u32[]{:S(2)}) copy-start(f32[256,256]{1,0:T(8,128)} %get-tuple-element.16.refs_0_) | copy-start | bytes 786436
  78.4 0.9 %copy-start.3 = (f32[256,256]{1,0:T(8,128)S(1)}, f32[256,256]{1,0:T(8,128)}, u32[]{:S(2)}) copy-start(f32[256,256]{1,0:T(8,128)} %get-tuple-element.17.refs_1_) | copy-start | bytes 786436
  79.4 0.9 %copy-start.4 = (f32[256,256]{1,0:T(8,128)S(1)}, f32[256,256]{1,0:T(8,128)}, u32[]{:S(2)}) copy-start(f32[256,256]{1,0:T(8,128)} %get-tuple-element.18.refs_2_) | copy-start | bytes 786436
  80.3 0.9 %copy-start.5 = (f32[256,256]{1,0:T(8,128)S(1)}, f32[256,256]{1,0:T(8,128)}, u32[]{:S(2)}) copy-start(f32[256,256]{1,0:T(8,128)} %get-tuple-element.19.refs_3_) | copy-start | bytes 786436
  81.3 0.9 %copy-start.6 = (f32[2,256,128]{2,1,0:T(8,128)S(1)}, f32[2,256,128]{2,1,0:T(8,128)}, u32[]{:S(2)}) copy-start(f32[2,256,128]{2,1,0:T(8,128)} %get-tuple-element.20.refs_4_) | copy-start | bytes 786436
  82.2 0.9 %copy-start.7 = (f32[2,256,128]{2,1,0:T(8,128)S(1)}, f32[2,256,128]{2,1,0:T(8,128)}, u32[]{:S(2)}) copy-start(f32[2,256,128]{2,1,0:T(8,128)} %get-tuple-element.21.refs_5_) | copy-start | bytes 786436

commit v3 on v2

--- a/solution.py
+++ b/solution.py
@@ -414,7 +414,7 @@
             out_specs=[vmem] * 8,
             scratch_shapes=scratch,
             compiler_params=pltpu.CompilerParams(
-                collective_id=0, has_side_effects=True, vmem_limit_bytes=54 * 1024 * 1024
+                collective_id=0, has_side_effects=True, vmem_limit_bytes=51 * 1024 * 1024
             ),
         )(saved_input, key_cot, mixed_out, out_cot, key_weight, out_weight, bases, first_moment, second_moment)
         return pl.pallas_call(

time: 85.5 us -> 82.8 us (0.968)
  local copies, waits for them, and re-layouts: 8.14 us -> 6.23 us
    unnamed x16 -> x12, local copies, waits for them, and re-layouts: 8.14 us -> 6.23 us
where the time goes in v3:
time: 82.8 us; the launch traced here: 82.5 us
  Pallas kernels  75.6 us (91%)
  local copies, waits for them, and re-layouts  6.23 us (8%)
    pallas_call x1, Pallas kernels, body(): pl.pallas_call(functools.partial(kernel, fs, tp), out_shape=outs, in_spec...  73.7 us
    unnamed x12, local copies, waits for them, and re-layouts  6.23 us
    pallas_call x1, Pallas kernels, body(): pl.pallas_call(move_out, out_shape=outs, in_specs=[pl.BlockSpec(memory_sp...  1.9 us

profile of v3, /device:TPU:0, one launch (start us, length us, event | category | flops | bytes accessed | tf_op | source)
XLA Modules:
  0.0 82.5 jit_solution(18411234711178917773)
XLA Ops:
  0.6 0.0 copy-start.2
  0.6 0.9 %copy-done.2 = f32[256,256]{1,0:T(8,128)S(1)} copy-done((f32[256,256]{1,0:T(8,128)S(1)}, f32[256,256]{1,0:T(8,128)}, u32[]{:S(2)}) %copy-start.2) | copy-done | bytes 262168
  1.6 0.0 copy-start.3
  1.6 0.9 %copy-done.3 = f32[256,256]{1,0:T(8,128)S(1)} copy-done((f32[256,256]{1,0:T(8,128)S(1)}, f32[256,256]{1,0:T(8,128)}, u32[]{:S(2)}) %copy-start.3) | copy-done | bytes 262168
  2.5 0.0 copy-start.4
  2.5 0.9 %copy-done.4 = f32[2,256,128]{2,1,0:T(8,128)S(1)} copy-done((f32[2,256,128]{2,1,0:T(8,128)S(1)}, f32[2,256,128]{2,1,0:T(8,128)}, u32[]{:S(2)}) %copy-start.4) | copy-done | bytes 262168
  3.5 0.0 copy-start.5
  3.5 0.9 %copy-done.5 = f32[2,256,128]{2,1,0:T(8,128)S(1)} copy-done((f32[2,256,128]{2,1,0:T(8,128)S(1)}, f32[2,256,128]{2,1,0:T(8,128)}, u32[]{:S(2)}) %copy-start.5) | copy-done | bytes 262168
  4.4 73.7 %shard_map.152 = (f32[256,256]{1,0:T(8,128)S(1)}, f32[256,256]{1,0:T(8,128)S(1)}, f32[256,256]{1,0:T(8,128)S(1)}, f32[256,256]{1,0:T(8,128)S(1)}, f32[2,256,128]...) custom-call(bf16[1536,2048]{1,0:T(8,128)(2,1)} %x0_hbm.1, ...), custom_call_target="tpu_custom_call" | custom-call | tf_op jit(solution)/shard_map/pallas_call | solution.py:410
  78.2 0.0 copy-start
  78.2 1.2 %copy-done = bf16[2048,256]{1,0:T(8,128)(2,1)S(1)} copy-done((bf16[2048,256]{1,0:T(8,128)(2,1)S(1)}, bf16[2048,256]{1,0:T(8,128)(2,1)}, u32[]{:S(2)}) %copy-start) | copy-done | bytes 1048600
  79.4 0.0 copy-start.1
  79.4 1.2 %copy-done.1 = bf16[256,2048]{1,0:T(8,128)(2,1)S(1)} copy-done((bf16[256,2048]{1,0:T(8,128)(2,1)S(1)}, bf16[256,2048]{1,0:T(8,128)(2,1)}, u32[]{:S(2)}) %copy-start.1) | copy-done | bytes 1048600
  80.6 1.9 %shard_map.153 = (f32[256,256]{1,0:T(8,128)}, f32[256,256]{1,0:T(8,128)}, f32[256,256]{1,0:T(8,128)}, f32[256,256]{1,0:T(8,128)}, f32[2,256,128]{2,1,0:T(8,128)}...) custom-call(f32[256,256]{1,0:T(8,128)S(1)} %get-tuple-element.16.refs_0_, ...), custom_call_target="tpu_custom_call" | custom-call | tf_op jit(solution)/shard_map/pallas_call | solution.py:420
Async XLA Ops:
  0.6 1.0 %copy-start.2 = (f32[256,256]{1,0:T(8,128)S(1)}, f32[256,256]{1,0:T(8,128)}, u32[]{:S(2)}) copy-start(f32[256,256]{1,0:T(8,128)} %key_w_hbm.1) | copy-start | bytes 786436
  1.6 0.9 %copy-start.3 = (f32[256,256]{1,0:T(8,128)S(1)}, f32[256,256]{1,0:T(8,128)}, u32[]{:S(2)}) copy-start(f32[256,256]{1,0:T(8,128)} %out_w_hbm.1) | copy-start | bytes 786436
  2.5 0.9 %copy-start.4 = (f32[2,256,128]{2,1,0:T(8,128)S(1)}, f32[2,256,128]{2,1,0:T(8,128)}, u32[]{:S(2)}) copy-start(f32[2,256,128]{2,1,0:T(8,128)} %first_hbm.1) | copy-start | bytes 786436
  3.5 0.9 %copy-start.5 = (f32[2,256,128]{2,1,0:T(8,128)S(1)}, f32[2,256,128]{2,1,0:T(8,128)}, u32[]{:S(2)}) copy-start(f32[2,256,128]{2,1,0:T(8,128)} %second_hbm.1) | copy-start | bytes 786436
  78.2 1.2 %copy-start = (bf16[2048,256]{1,0:T(8,128)(2,1)S(1)}, bf16[2048,256]{1,0:T(8,128)(2,1)}, u32[]{:S(2)}) copy-start(bf16[2048,256]{1,0:T(8,128)(2,1)} %get-tuple-element.22.refs_6_) | copy-start | bytes 3145732
  79.4 1.2 %copy-start.1 = (bf16[256,2048]{1,0:T(8,128)(2,1)S(1)}, bf16[256,2048]{1,0:T(8,128)(2,1)}, u32[]{:S(2)}) copy-start(bf16[256,2048]{1,0:T(8,128)(2,1)} %get-tuple-element.23.refs_7_) | copy-start | bytes 3145732

commit v4 on v3

--- a/solution.py
+++ b/solution.py
@@ -414,7 +414,7 @@
             out_specs=[vmem] * 8,
             scratch_shapes=scratch,
             compiler_params=pltpu.CompilerParams(
-                collective_id=0, has_side_effects=True, vmem_limit_bytes=51 * 1024 * 1024
+                collective_id=0, has_side_effects=True, vmem_limit_bytes=(48 if Q >= 128 else 54) * 1024 * 1024
             ),
         )(saved_input, key_cot, mixed_out, out_cot, key_weight, out_weight, bases, first_moment, second_moment)
         return pl.pallas_call(

time: 82.8 us -> 79 us (0.954)
  local copies, waits for them, and re-layouts: 6.23 us -> 3.79 us
  Pallas kernels: 75.6 us -> 74.3 us
    unnamed x12 -> x8, local copies, waits for them, and re-layouts: 6.23 us -> 3.79 us
    pallas_call x1, Pallas kernels: 73.7 us -> 72.4 us  [body(): pl.pallas_call(functools.partial(kernel, fs, tp), out_shape=outs, in_spec...]
where the time goes in v4:
time: 79 us; the launch traced here: 78.7 us
  Pallas kernels  74.3 us (94%)
  local copies, waits for them, and re-layouts  3.79 us (5%)
    pallas_call x1, Pallas kernels, body(): pl.pallas_call(functools.partial(kernel, fs, tp), out_shape=outs, in_spec...  72.4 us
    unnamed x8, local copies, waits for them, and re-layouts  3.79 us
    pallas_call x1, Pallas kernels, body(): pl.pallas_call(move_out, out_shape=outs, in_specs=[pl.BlockSpec(memory_sp...  1.91 us

profile of v4, /device:TPU:0, one launch (start us, length us, event | category | flops | bytes accessed | tf_op | source)
XLA Modules:
  0.0 78.7 jit_solution(10127484427974516209)
XLA Ops:
  0.6 0.0 copy-start
  0.6 0.9 %copy-done = f32[256,256]{1,0:T(8,128)S(1)} copy-done((f32[256,256]{1,0:T(8,128)S(1)}, f32[256,256]{1,0:T(8,128)}, u32[]{:S(2)}) %copy-start) | copy-done | bytes 262168
  1.6 0.0 copy-start.1
  1.6 0.9 %copy-done.1 = f32[256,256]{1,0:T(8,128)S(1)} copy-done((f32[256,256]{1,0:T(8,128)S(1)}, f32[256,256]{1,0:T(8,128)}, u32[]{:S(2)}) %copy-start.1) | copy-done | bytes 262168
  2.5 0.0 copy-start.2
  2.5 0.9 %copy-done.2 = f32[2,256,128]{2,1,0:T(8,128)S(1)} copy-done((f32[2,256,128]{2,1,0:T(8,128)S(1)}, f32[2,256,128]{2,1,0:T(8,128)}, u32[]{:S(2)}) %copy-start.2) | copy-done | bytes 262168
  3.5 0.0 copy-start.3
  3.5 0.9 %copy-done.3 = f32[2,256,128]{2,1,0:T(8,128)S(1)} copy-done((f32[2,256,128]{2,1,0:T(8,128)S(1)}, f32[2,256,128]{2,1,0:T(8,128)}, u32[]{:S(2)}) %copy-start.3) | copy-done | bytes 262168
  4.4 72.4 %shard_map.152 = (f32[256,256]{1,0:T(8,128)S(1)}, f32[256,256]{1,0:T(8,128)S(1)}, f32[256,256]{1,0:T(8,128)S(1)}, f32[256,256]{1,0:T(8,128)S(1)}, f32[2,256,128]...) custom-call(bf16[1536,2048]{1,0:T(8,128)(2,1)} %x0_hbm.1, ...), custom_call_target="tpu_custom_call" | custom-call | tf_op jit(solution)/shard_map/pallas_call | solution.py:410
  76.8 1.9 %shard_map.153 = (f32[256,256]{1,0:T(8,128)}, f32[256,256]{1,0:T(8,128)}, f32[256,256]{1,0:T(8,128)}, f32[256,256]{1,0:T(8,128)}, f32[2,256,128]{2,1,0:T(8,128)}...) custom-call(f32[256,256]{1,0:T(8,128)S(1)} %get-tuple-element.16.refs_0_, ...), custom_call_target="tpu_custom_call" | custom-call | tf_op jit(solution)/shard_map/pallas_call | solution.py:420
Async XLA Ops:
  0.6 1.0 %copy-start = (f32[256,256]{1,0:T(8,128)S(1)}, f32[256,256]{1,0:T(8,128)}, u32[]{:S(2)}) copy-start(f32[256,256]{1,0:T(8,128)} %key_w_hbm.1) | copy-start | bytes 786436
  1.6 0.9 %copy-start.1 = (f32[256,256]{1,0:T(8,128)S(1)}, f32[256,256]{1,0:T(8,128)}, u32[]{:S(2)}) copy-start(f32[256,256]{1,0:T(8,128)} %out_w_hbm.1) | copy-start | bytes 786436
  2.5 0.9 %copy-start.2 = (f32[2,256,128]{2,1,0:T(8,128)S(1)}, f32[2,256,128]{2,1,0:T(8,128)}, u32[]{:S(2)}) copy-start(f32[2,256,128]{2,1,0:T(8,128)} %first_hbm.1) | copy-start | bytes 786436
  3.5 0.9 %copy-start.3 = (f32[2,256,128]{2,1,0:T(8,128)S(1)}, f32[2,256,128]{2,1,0:T(8,128)}, u32[]{:S(2)}) copy-start(f32[2,256,128]{2,1,0:T(8,128)} %second_hbm.1) | copy-start | bytes 786436
